TPU v7x, 32 devices: a whole 2x2x4 slice. The times are simulated.
32 devices in a mesh: fs: 4 (over z), tp: 8 (over y, x, core).
Axes of the slice: x: 2, y: 2, z: 4, core: 2. Of those that a mesh axis runs over, the one named last changes fastest.
Arguments:
- tokens: bfloat16 [768, 2304], P('fs'), may hold values from -6 to 6
- gate_train: float32 [8, 2304, 2304], P(None, 'fs', 'tp'), may hold values from -0.125 to 0.125
- up_train: float32 [8, 2304, 2304], P(None, 'fs', 'tp'), may hold values from -0.125 to 0.125
- down_train: float32 [8, 2304, 2304], P(None, 'fs', 'tp'), may hold values from -0.125 to 0.125
- gain: float32 [2304], P('fs'), may hold values from 0.1 to 1.9
- routes: int32 [768, 2], P('fs'), may hold values from 0 to 7, all different within a row; in each aligned block of 192 rows (0 to 191, 192 to 383, ...) at most 72 rows name the same one
- route_weights: float32 [768, 2], P('fs'), may hold values from 0.1 to 1
Outputs:
- gate_new: bfloat16 [8, 2304, 2304], P('tp')
- up_new: bfloat16 [8, 2304, 2304], P('tp')
- down_new: bfloat16 [8, 2304, 2304], P('tp')
- mixed: bfloat16 [768, 2304], P('fs', 'tp')
Inputs may be any that keep to these rules, and one draw needn't show every extreme that they name: `routes`: each row names two different experts; in each aligned block of 192 rows at most 72 rows name one expert, a bound that some block reaches.
All inputs are finite; a program needn't handle non-finite values.
Results may differ from a plain program's by a relative error of at most 0.0095.
Values may be sent and summed in bfloat16 or wider, within the bound.
A program may use at most 128 MiB of HBM per device.

v0:
```python
import jax
import jax.numpy as jnp
from jax import lax
from jax.sharding import PartitionSpec as P

CAP = 72
norm_eps = 1e-06


def arrange(matrix, tp_count):
    experts, row_count, col_count = matrix.shape
    slices = tp_count // experts
    piece_width = col_count // slices
    shaped = matrix.reshape(experts, row_count, slices, piece_width)
    return shaped.transpose(0, 2, 3, 1).reshape(tp_count, piece_width, row_count)


def shards(tokens, gate_train, up_train, down_train, gain, routes, route_weights):
    tp_count = lax.axis_size("tp")
    experts = gate_train.shape[0]
    slices = tp_count // experts
    gain_column = gain[None, :, None]
    gate_round = (gate_train * gain_column).astype(jnp.bfloat16)
    up_round = (up_train * gain_column).astype(jnp.bfloat16)
    down_round = down_train.astype(jnp.bfloat16)
    moved = (
        lax.all_to_all(
            arrange(gate_round, tp_count), "tp", split_axis=0, concat_axis=1, tiled=True
        ),
        lax.all_to_all(arrange(up_round, tp_count), "tp", split_axis=0, concat_axis=1, tiled=True),
        lax.all_to_all(
            arrange(down_round, tp_count), "tp", split_axis=0, concat_axis=1, tiled=True
        ),
    )
    tokens_wide = tokens.astype(jnp.float32)
    normed = (
        tokens_wide
        * lax.rsqrt(jnp.mean(tokens_wide * tokens_wide, axis=1, keepdims=True) + norm_eps)
    ).astype(jnp.bfloat16)
    expert = lax.axis_index("tp") // slices
    matches = routes == expert
    member = jnp.any(matches, axis=1)
    slot_index = jnp.cumsum(member.astype(jnp.int32)) - 1
    marked = jnp.where(member, slot_index, -1)
    picker = (marked[None, :] == jnp.arange(CAP, dtype=jnp.int32)[:, None]).astype(jnp.bfloat16)
    chosen = jnp.dot(picker, normed, preferred_element_type=jnp.float32).astype(jnp.bfloat16)
    contract_last = (((1,), (1,)), ((), ()))
    gate_new, up_new, down_new = (
        lax.all_gather(moved[0], "fs", axis=2, tiled=True),
        lax.all_gather(moved[1], "fs", axis=2, tiled=True),
        lax.all_gather(moved[2], "fs", axis=2, tiled=True),
    )
    gate_pre = lax.dot_general(
        chosen, gate_new[0], contract_last, preferred_element_type=jnp.float32
    )
    up_pre = lax.dot_general(chosen, up_new[0], contract_last, preferred_element_type=jnp.float32)
    hidden = (jax.nn.silu(gate_pre) * up_pre).astype(jnp.bfloat16)
    partial_value = jnp.dot(hidden, down_new[0], preferred_element_type=jnp.float32).astype(
        jnp.bfloat16
    )
    labels = jnp.arange(experts, dtype=jnp.int32)
    member_all = jnp.any(routes[:, :, None] == labels[None, None, :], axis=1)
    slots_all = jnp.cumsum(member_all.astype(jnp.int32), axis=0) - 1
    slot_pair = jnp.take_along_axis(slots_all, routes, axis=1)
    flat_index = slot_pair * experts + routes
    received = lax.all_to_all(
        partial_value.reshape(CAP, tp_count, -1), "tp", split_axis=1, concat_axis=1, tiled=True
    )
    summed = jnp.sum(received.reshape(CAP, experts, slices, -1).astype(jnp.float32), axis=2)
    summed = summed.reshape(CAP * experts, -1)
    picked = jnp.take(summed, flat_index, axis=0)
    mixed = jnp.sum(route_weights[:, :, None] * picked, axis=1)
    return (gate_new, up_new, down_new, mixed.astype(jnp.bfloat16))


def solution(mesh):
    in_specs = (
        P("fs", None),
        P(None, "fs", "tp"),
        P(None, "fs", "tp"),
        P(None, "fs", "tp"),
        P("fs"),
        P("fs", None),
        P("fs", None),
    )
    out_specs = (P("tp", None, None), P("tp", None, None), P("tp", None, None), P("fs", "tp"))
    return jax.shard_map(shards, mesh=mesh, in_specs=in_specs, out_specs=out_specs, check_vma=False)
```

profile of v0, /device:TPU:1, one launch (start us, length us, event | category | flops | bytes accessed | tf_op | source)
XLA Modules:
  0.0 690.3 jit_solution(4470130244694976679)
XLA Ops:
  7.2 0.0 all-gather.4.cloned.1.call-start
  7.2 5.4 fusion.16
  12.6 40.1 %all_to_all.41 = bf16[8,288,576]{2,1,0:T(8,128)(2,1)} all-to-all(bf16[8,288,576]{2,1,0:T(8,128)(2,1)S(1)} %get-tuple-element.23), channel_id=1, replica_groups=mesh['fs'=4,'tp'=8] {'tp'}, dimensions={0} | all-to-all | bytes 5308416 | tf_op jit(solution)/shard_map/all_to_all | solution.py:27
  52.6 4.5 copy.89
  57.1 0.0 all-gather.4.cloned.1.call-update
  57.1 0.0 all-gather.6.cloned.1.call-start
  57.2 39.1 %all_to_all.42 = bf16[8,288,576]{2,1,0:T(8,128)(2,1)} all-to-all(bf16[8,288,576]{2,1,0:T(8,128)(2,1)S(1)} %get-tuple-element.22), channel_id=1, replica_groups=mesh['fs'=4,'tp'=8] {'tp'}, dimensions={0} | all-to-all | bytes 5308416 | tf_op jit(solution)/shard_map/all_to_all | solution.py:30
  96.3 4.5 copy.90
  100.8 0.0 all-gather.6.cloned.1.call-update
  100.8 0.0 all-gather.8.cloned.1.call-start
  100.9 3.0 convert_bitcast_fusion
  103.9 0.0 copy-start.1
  103.9 38.2 %all_to_all.43 = bf16[8,288,576]{2,1,0:T(8,128)(2,1)S(1)} all-to-all(bf16[8,288,576]{2,1,0:T(8,128)(2,1)S(1)} %convert_bitcast_fusion), channel_id=1, replica_groups=mesh['fs'=4,'tp'=8] {'tp'}, dimensions={0} | all-to-all | bytes 5308416 | tf_op jit(solution)/shard_map/all_to_all | solution.py:31
  142.2 3.4 copy.91
  145.5 0.0 all-gather.8.cloned.1.call-update
  145.6 0.0 copy-done.1
  145.6 0.6 reduce-window.15
  146.2 0.2 slice_reduce_fusion
  146.5 0.1 copy.93
  146.6 0.1 reshape.127
  146.7 0.1 add_bitcast_fusion
  146.8 0.0 copy-start
  146.8 2.7 gather_fusion.1
  149.5 0.1 reshape.130
  149.6 0.1 copy.94
  149.8 0.3 reduce-window.19
  150.1 0.1 slice.22
  150.2 0.1 slice_reduce_fusion.1
  150.3 0.0 copy-done
  150.3 0.3 fusion.17
  150.6 0.1 add_bitcast_fusion.1
  150.6 0.4 convolution_convert_fusion
  151.0 91.9 %all-gather.4.cloned.1.call-done = bf16[1,2304,2304]{1,2,0:T(8,128)(2,1)} async-done(((bf16[1,2304,576]{1,2,0:T(8,128)(2,1)}), bf16[1,2304,2304]{1,2,0:T(8,128)(2,1)}) %all-gather.4.cloned.1.call-update) | async-done | bytes 10616848 | tf_op jit(solution)/shard_map/all_gather | solution.py:49
  242.9 6.0 fusion.4
  248.9 0.0 copy-start.2
  249.0 180.4 %all-gather.6.cloned.1.call-done = bf16[1,2304,2304]{1,2,0:T(8,128)(2,1)} async-done(((bf16[1,2304,576]{1,2,0:T(8,128)(2,1)}), bf16[1,2304,2304]{1,2,0:T(8,128)(2,1)}) %all-gather.6.cloned.1.call-update) | async-done | bytes 10616848 | tf_op jit(solution)/shard_map/all_gather | solution.py:50
  429.4 186.4 %all-gather.8.cloned.1.call-done = bf16[1,2304,2304]{1,2,0:T(8,128)(2,1)} async-done(((bf16[1,2304,576]{1,2,0:T(8,128)(2,1)}), bf16[1,2304,2304]{1,2,0:T(8,128)(2,1)}) %all-gather.8.cloned.1.call-update) | async-done | bytes 10616848 | tf_op jit(solution)/shard_map/all_gather | solution.py:51
  615.8 11.9 %fusion.12 = bf16[72,2304]{1,0:T(8,128)(2,1)S(1)} fusion(bf16[1,2304,2304]{1,2,0:T(8,128)(2,1)} %all-gather.8.cloned.1.call-done, bf16[72,2304]{1,0:T(8,128)(2,1)S(1)} %convolution_convert_fusion, bf16[1,2304,2304]{1,2,0:T(8,128)(2,1)} %all-gather.6.cloned.1.call-done, f32[72,2304]{1,0:T(8,128)S(1)} %fusion.4), kind=kOutput, calls=%fused_computation.12 | convolution fusion | flops 1529985024 | bytes 22560768 | tf_op jit(solution)/shard_map/dot_general | solution.py:58
  627.7 0.7 reshape.112
  628.4 0.8 copy.96
  629.2 4.2 all-to-all-start.3
  633.3 0.1 copy.98
  633.5 0.1 reshape.121
  633.6 0.2 copy.95
  633.8 0.0 copy-done.2
  633.8 0.1 copy.92
  633.9 15.2 %copy.100 = bf16[1,2304,2304]{2,1,0:T(8,128)(2,1)} copy(bf16[1,2304,2304]{1,2,0:T(8,128)(2,1)} %all-gather.6.cloned.1.call-done) | data formatting | bytes 21233664
  649.1 15.2 %copy.99 = bf16[1,2304,2304]{2,1,0:T(8,128)(2,1)} copy(bf16[1,2304,2304]{1,2,0:T(8,128)(2,1)} %all-gather.4.cloned.1.call-done) | data formatting | bytes 21233664
  664.4 15.2 %copy.101 = bf16[1,2304,2304]{2,1,0:T(8,128)(2,1)} copy(bf16[1,2304,2304]{1,2,0:T(8,128)(2,1)} %all-gather.8.cloned.1.call-done) | data formatting | bytes 21233664
  679.6 0.0 all-to-all-done.3
  679.6 0.1 copy.103
  679.6 1.7 gather_fusion
  681.4 0.3 reshape.120
  681.7 2.0 multiply_reduce_fusion
  (12 shorter events, 0.2 us)
Async XLA Ops:
  7.2 235.8 %all-gather.4.cloned.1.call-start = ((), (), s32[]{:S(2)}) async-start(), calls=%async_computation.4 | async-start | bytes 13271040 | tf_op jit(solution)/shard_map/all_gather | solution.py:49
  57.1 372.2 %all-gather.6.cloned.1.call-start = ((), (), s32[]{:S(2)}) async-start(), calls=%async_computation.5 | async-start | bytes 13271040 | tf_op jit(solution)/shard_map/all_gather | solution.py:50
  100.8 514.9 %all-gather.8.cloned.1.call-start = ((), (), s32[]{:S(2)}) async-start(), calls=%async_computation.6 | async-start | bytes 13271040 | tf_op jit(solution)/shard_map/all_gather | solution.py:51
  103.9 41.7 %copy-start.1 = (s32[192,2]{0,1:T(2,128)S(1)}, s32[192,2]{0,1:T(2,128)}, u32[]{:S(2)}) copy-start(s32[192,2]{0,1:T(2,128)} %param.12) | copy-start | bytes 4612
  146.8 3.5 copy-start
  248.9 384.8 %copy-start.2 = (f32[192,2]{0,1:T(2,128)S(1)}, f32[192,2]{0,1:T(2,128)}, u32[]{:S(2)}) copy-start(f32[192,2]{0,1:T(2,128)} %param.13) | copy-start | bytes 4612
  629.2 50.4 %all-to-all-start.3 = ((bf16[72,8,288]{2,0,1:T(8,128)(2,1)}), bf16[72,8,288]{2,0,1:T(8,128)(2,1)S(1)}, u32[]{:S(2)}, u32[]{:S(2)}) async-start(bf16[72,8,288]{2,0,1:T(8,128)(2,1)} %copy.96), calls=%async_computation.3 | async-start | bytes 884736 | tf_op jit(solution)/shard_map/all_to_all | solution.py:66
Sparse Core Ops, SparseCore 0:
  57.3 185.6 all-gather.3
  245.1 184.2 all-gather.5
  431.5 184.2 all-gather.7
where the time goes:
time: 692 us; the launch traced here: 690 us
  waiting for transfers between devices  459 us (66%)
  blocking collectives  117 us (17%)
  local copies, waits for them, and re-layouts  65.7 us (9%)
  matrix products  18.3 us (3%)
  between operations  13.9 us (2%)
  other arithmetic  11.9 us (2%)
    all_gather x1, waiting for transfers between devices, shards(): lax.all_gather(moved[2], 'fs', axis=2, tiled=True)  186 us
    all_gather x1, waiting for transfers between devices, shards(): lax.all_gather(moved[1], 'fs', axis=2, tiled=True)  180 us
    all_gather x1, waiting for transfers between devices, shards(): lax.all_gather(moved[0], 'fs', axis=2, tiled=True)  91.9 us
    unnamed x10, local copies, waits for them, and re-layouts  45.8 us
    all_to_all x1, blocking collectives, shards(): lax.all_to_all(arrange(gate_round, tp_count), 'tp', split_axis=0, concat_...  40.1 us
    all_to_all x1, blocking collectives, shards(): lax.all_to_all(arrange(up_round, tp_count), 'tp', split_axis=0, concat_ax...  39.1 us
    all_to_all x1, blocking collectives, shards(): lax.all_to_all(arrange(down_round, tp_count), 'tp', split_axis=0, concat_...  38.2 us
  transfers between devices with their start and end apart: 4, of which 3 were waited for; matrix products, arithmetic and copies ran while one was open for 10% of the time, Pallas kernels for 0%

commit v1 on v0

--- a/solution.py
+++ b/solution.py
@@ -47,7 +47,7 @@
     contract_last = (((1,), (1,)), ((), ()))
     gate_new, up_new, down_new = (
         lax.all_gather(moved[0], "fs", axis=2, tiled=True),
-        lax.all_gather(moved[1], "fs", axis=2, tiled=True),
+        jnp.concatenate(lax.all_gather(moved[1], "fs"), axis=2),
         lax.all_gather(moved[2], "fs", axis=2, tiled=True),
     )
     gate_pre = lax.dot_general(

time: 692 us -> 692 us (level)
  no operation moved by 1% of the time
where the time goes in v1:
time: 692 us; the launch traced here: 690 us
  waiting for transfers between devices  459 us (66%)
  blocking collectives  117 us (17%)
  local copies, waits for them, and re-layouts  65.7 us (9%)
  matrix products  18.3 us (3%)
  between operations  13.9 us (2%)
  other arithmetic  11.9 us (2%)
    all_gather x1, waiting for transfers between devices, shards(): lax.all_gather(moved[2], 'fs', axis=2, tiled=True)  186 us
    all_gather x1, waiting for transfers between devices, shards(): lax.all_gather(moved[1], 'fs')  180 us
    all_gather x1, waiting for transfers between devices, shards(): lax.all_gather(moved[0], 'fs', axis=2, tiled=True)  91.9 us
    unnamed x10, local copies, waits for them, and re-layouts  45.8 us
    all_to_all x1, blocking collectives, shards(): lax.all_to_all(arrange(gate_round, tp_count), 'tp', split_axis=0, concat_...  40.1 us
    all_to_all x1, blocking collectives, shards(): lax.all_to_all(arrange(up_round, tp_count), 'tp', split_axis=0, concat_ax...  39.1 us
    all_to_all x1, blocking collectives, shards(): lax.all_to_all(arrange(down_round, tp_count), 'tp', split_axis=0, concat_...  38.2 us
  transfers between devices with their start and end apart: 4, of which 3 were waited for; matrix products, arithmetic and copies ran while one was open for 10% of the time, Pallas kernels for 0%

profile of v1, /device:TPU:1, one launch (start us, length us, event | category | flops | bytes accessed | tf_op | source)
XLA Modules:
  0.0 690.3 jit_solution(16407702111998568048)
XLA Ops:
  7.2 0.0 all-gather.4.cloned.1.call-start
  7.2 5.4 fusion.9
  12.6 40.1 %all_to_all.38 = bf16[8,288,576]{2,1,0:T(8,128)(2,1)} all-to-all(bf16[8,288,576]{2,1,0:T(8,128)(2,1)S(1)} %get-tuple-element.31), channel_id=1, replica_groups=mesh['fs'=4,'tp'=8] {'tp'}, dimensions={0} | all-to-all | bytes 5308416 | tf_op jit(solution)/shard_map/all_to_all | solution.py:27
  52.6 4.5 copy.111
  57.1 0.0 all-gather.4.cloned.1.call-update
  57.1 0.0 all-gather.6.cloned.1.call-start
  57.2 39.1 %all_to_all.39 = bf16[8,288,576]{2,1,0:T(8,128)(2,1)} all-to-all(bf16[8,288,576]{2,1,0:T(8,128)(2,1)S(1)} %get-tuple-element.30), channel_id=1, replica_groups=mesh['fs'=4,'tp'=8] {'tp'}, dimensions={0} | all-to-all | bytes 5308416 | tf_op jit(solution)/shard_map/all_to_all | solution.py:30
  96.3 4.5 copy.112
  100.8 0.0 all-gather.6.cloned.1.call-update
  100.8 0.0 all-gather.8.cloned.1.call-start
  100.9 3.0 convert_bitcast_fusion
  103.9 0.0 copy-start.1
  103.9 38.2 %all_to_all.40 = bf16[8,288,576]{2,1,0:T(8,128)(2,1)S(1)} all-to-all(bf16[8,288,576]{2,1,0:T(8,128)(2,1)S(1)} %convert_bitcast_fusion), channel_id=1, replica_groups=mesh['fs'=4,'tp'=8] {'tp'}, dimensions={0} | all-to-all | bytes 5308416 | tf_op jit(solution)/shard_map/all_to_all | solution.py:31
  142.2 3.4 copy.114
  145.5 0.0 all-gather.8.cloned.1.call-update
  145.6 0.0 copy-done.1
  145.6 0.6 reduce-window.15
  146.2 0.2 slice_reduce_fusion
  146.5 0.1 copy.116
  146.6 0.1 reshape.136
  146.7 0.1 add_bitcast_fusion
  146.8 0.0 copy-start
  146.8 2.7 gather_fusion.1
  149.5 0.1 reshape.139
  149.6 0.1 copy.117
  149.8 0.3 reduce-window.19
  150.1 0.1 slice.22
  150.2 0.1 slice_reduce_fusion.1
  150.3 0.0 copy-done
  150.3 0.3 fusion.10
  150.6 0.1 add_bitcast_fusion.1
  150.6 0.4 convolution_convert_fusion
  151.0 91.9 %all-gather.4.cloned.1.call-done = bf16[1,2304,2304]{1,2,0:T(8,128)(2,1)} async-done(((bf16[1,2304,576]{1,2,0:T(8,128)(2,1)}), bf16[1,2304,2304]{1,2,0:T(8,128)(2,1)}) %all-gather.4.cloned.1.call-update) | async-done | bytes 10616848 | tf_op jit(solution)/shard_map/all_gather | solution.py:49
  242.9 6.0 fusion.2
  248.9 180.4 %all-gather.6.cloned.1.call-done = bf16[4,1,2304,576]{2,3,1,0:T(8,128)(2,1)} async-done(((bf16[1,1,2304,576]{2,3,1,0:T(8,128)(2,1)}), bf16[4,1,2304,576]{2,3,1,0:T(8,128)(2,1)}) %all-gather.6.cloned.1.call-update) | async-done | bytes 10616848 | tf_op jit(solution)/shard_map/all_gather | solution.py:50
  429.4 186.4 %all-gather.8.cloned.1.call-done = bf16[1,2304,2304]{1,2,0:T(8,128)(2,1)} async-done(((bf16[1,2304,576]{1,2,0:T(8,128)(2,1)}), bf16[1,2304,2304]{1,2,0:T(8,128)(2,1)}) %all-gather.8.cloned.1.call-update) | async-done | bytes 10616848 | tf_op jit(solution)/shard_map/all_gather | solution.py:51
  615.8 0.0 copy-start.2
  615.8 11.9 %fusion.5 = bf16[72,2304]{1,0:T(8,128)(2,1)S(1)} fusion(bf16[1,2304,2304]{1,2,0:T(8,128)(2,1)} %all-gather.8.cloned.1.call-done, bf16[72,2304]{1,0:T(8,128)(2,1)S(1)} %convolution_convert_fusion, bf16[2304,2304]{0,1:T(8,128)(2,1)} %bitcast.57, f32[72,2304]{1,0:T(8,128)S(1)} %fusion.2), kind=kOutput, calls=%fused_computation.10 | convolution fusion | flops 1529985024 | bytes 22560768 | tf_op jit(solution)/shard_map/dot_general | solution.py:58
  627.7 0.7 reshape.121
  628.4 0.8 copy.119
  629.2 4.2 all-to-all-start.3
  633.4 0.1 copy.121
  633.5 0.1 reshape.130
  633.6 0.2 copy.118
  633.8 0.0 copy-done.2
  633.8 0.1 copy.115
  633.9 15.2 %copy.123 = bf16[1,2304,2304]{2,1,0:T(8,128)(2,1)} copy(bf16[1,2304,2304]{1,2,0:T(8,128)(2,1)} %bitcast.58) | data formatting | bytes 21233664
  649.2 15.2 %copy.122 = bf16[1,2304,2304]{2,1,0:T(8,128)(2,1)} copy(bf16[1,2304,2304]{1,2,0:T(8,128)(2,1)} %all-gather.4.cloned.1.call-done) | data formatting | bytes 21233664
  664.4 15.2 %copy.124 = bf16[1,2304,2304]{2,1,0:T(8,128)(2,1)} copy(bf16[1,2304,2304]{1,2,0:T(8,128)(2,1)} %all-gather.8.cloned.1.call-done) | data formatting | bytes 21233664
  679.6 0.0 all-to-all-done.3
  679.6 0.1 copy.126
  679.6 1.7 gather_fusion
  681.4 0.3 reshape.129
  681.7 2.0 multiply_reduce_fusion
  (12 shorter events, 0.2 us)
Async XLA Ops:
  7.2 235.8 %all-gather.4.cloned.1.call-start = ((), (), s32[]{:S(2)}) async-start(), calls=%async_computation.4 | async-start | bytes 13271040 | tf_op jit(solution)/shard_map/all_gather | solution.py:49
  57.1 372.2 %all-gather.6.cloned.1.call-start = ((), (), s32[]{:S(2)}) async-start(), calls=%async_computation.5 | async-start | bytes 13271040 | tf_op jit(solution)/shard_map/all_gather | solution.py:50
  100.8 514.9 %all-gather.8.cloned.1.call-start = ((), (), s32[]{:S(2)}) async-start(), calls=%async_computation.6 | async-start | bytes 13271040 | tf_op jit(solution)/shard_map/all_gather | solution.py:51
  103.9 41.7 %copy-start.1 = (s32[192,2]{0,1:T(2,128)S(1)}, s32[192,2]{0,1:T(2,128)}, u32[]{:S(2)}) copy-start(s32[192,2]{0,1:T(2,128)} %param.12) | copy-start | bytes 4612
  146.8 3.5 copy-start
  615.8 18.0 %copy-start.2 = (f32[192,2]{0,1:T(2,128)S(1)}, f32[192,2]{0,1:T(2,128)}, u32[]{:S(2)}) copy-start(f32[192,2]{0,1:T(2,128)} %param.13) | copy-start | bytes 4612
  629.2 50.4 %all-to-all-start.3 = ((bf16[72,8,288]{2,0,1:T(8,128)(2,1)}), bf16[72,8,288]{2,0,1:T(8,128)(2,1)S(1)}, u32[]{:S(2)}, u32[]{:S(2)}) async-start(bf16[72,8,288]{2,0,1:T(8,128)(2,1)} %copy.119), calls=%async_computation.3 | async-start | bytes 884736 | tf_op jit(solution)/shard_map/all_to_all | solution.py:66
Sparse Core Ops, SparseCore 0:
  57.3 185.6 all-gather.3
  245.1 184.2 all-gather.5
  431.5 184.2 all-gather.7
